TPU v7x, 32 devices: a whole 2x2x4 slice. The times are simulated.
32 devices in a mesh: sp: 8 (over z, core), tp: 4 (over y, x).
Axes of the slice: x: 2, y: 2, z: 4, core: 2. Of those that a mesh axis runs over, the one named last changes fastest.
Arguments:
- query_heads: bfloat16 [2048, 1024], P('sp', 'tp'), may hold values from -6 to 6
- key_heads: bfloat16 [2048, 256], P('sp'), may hold values from -6 to 6
- value_heads: bfloat16 [2048, 256], P('sp'), may hold values from -24 to 24
- q_gain: float32 [64], replicated, may hold values from 0.6 to 4.5
- k_gain: float32 [64], replicated, may hold values from 0.6 to 4.5
- out_weight: bfloat16 [1024, 2048], P('tp'), may hold values from -0.1875 to 0.1875
- residual: bfloat16 [2048, 2048], P('sp', 'tp'), may hold values from -3 to 3
- norm_gain: float32 [2048], P('tp'), may hold values from 0.1 to 1.9
- routes: int32 [2048, 2], P('sp'), may hold values from 0 to 7, all different within a row; in each aligned block of 256 rows (0 to 255, 256 to 511, ...) at most 81 rows name the same one
- route_weights: float32 [2048, 2], P('sp'), may hold values from 0.5 to 1.5
- w_gate: bfloat16 [8, 2048, 4096], P('sp', None, 'tp'), may hold values from -0.125 to 0.125
- w_up: bfloat16 [8, 2048, 4096], P('sp', None, 'tp'), may hold values from -0.125 to 0.125
- w_down: bfloat16 [8, 4096, 2048], P('sp', 'tp'), may hold values from -0.1875 to 0.1875
Outputs:
- layer_out: bfloat16 [2048, 2048], P('sp', 'tp')
Inputs may be any that keep to these rules, and one draw needn't show every extreme that they name: `routes`: each row names 2 different experts. Among the 256 rows of one index of sp, no expert is named more than 81 times, a bound that some block reaches.
All inputs are finite; a program needn't handle non-finite values.
Results may differ from a plain program's by a relative error of at most 0.02.
The roundings to bfloat16 on the way count: a program that leaves them out, or rounds other values in their place, can miss the bound.
Values may be sent and summed in bfloat16 or wider, within the bound.
No kernel may reach another device: no remote copies, remote signals or barrier semaphores. Data moves between devices by JAX's collectives and lax.ppermute only.
A program may use at most 64 MiB of HBM per device.

v0:
```python
import jax
import jax.numpy as jnp
from jax import lax
from jax.sharding import PartitionSpec as P

D = 2048
HQ = 16
KV = 4
E = 64
TOPK = 2
GRID_W = 64
norm_eps = 1e-06
rope_base = 10000.0


def normalize(values_f, gain):
    mean_sq = jnp.mean(values_f * values_f, axis=-1, keepdims=True)
    return values_f * lax.rsqrt(mean_sq + norm_eps) * gain


def rotate(values_f, positions):
    head_width = values_f.shape[-1]
    half_width = head_width // 2
    quarter_width = half_width // 2
    frequency = rope_base ** (-jnp.arange(quarter_width, dtype=jnp.float32) / quarter_width)
    grid_rows = (positions // GRID_W).astype(jnp.float32)
    grid_cols = (positions % GRID_W).astype(jnp.float32)
    shape = (values_f.shape[0],) + (1,) * (values_f.ndim - 2) + (quarter_width,)
    pieces = []
    for coords, offset_lo in ((grid_rows, 0), (grid_cols, half_width)):
        angles = coords[:, None] * frequency[None, :]
        cosine = jnp.cos(angles).reshape(shape)
        sines = jnp.sin(angles).reshape(shape)
        first_part = values_f[..., offset_lo : offset_lo + quarter_width]
        second_part = values_f[..., offset_lo + quarter_width : offset_lo + half_width]
        pieces.append(first_part * cosine - second_part * sines)
        pieces.append(second_part * cosine + first_part * sines)
    return jnp.concatenate(pieces, axis=-1)


def shards(
    query_heads,
    key_heads,
    value_heads,
    q_gain,
    k_gain,
    out_weight,
    residual,
    norm_gain,
    routes,
    route_weights,
    w_gate,
    w_up,
    w_down,
):
    tok_rows = query_heads.shape[0]
    head_local = query_heads.shape[1] // E
    group_size = HQ // KV
    kv_count = max(head_local // group_size, 1)
    per_kv = head_local // kv_count
    tp_index = lax.axis_index("tp")
    sp_index = lax.axis_index("sp")
    kv_first = tp_index * head_local // group_size
    positions = sp_index * tok_rows + jnp.arange(tok_rows, dtype=jnp.int32)
    query_f = query_heads.astype(jnp.float32).reshape(tok_rows, kv_count, per_kv, E)
    q_turned = rotate(normalize(query_f, q_gain), positions).astype(jnp.bfloat16)
    key_cols = lax.dynamic_slice_in_dim(key_heads, kv_first * E, kv_count * E, 1)
    value_cols = lax.dynamic_slice_in_dim(value_heads, kv_first * E, kv_count * E, 1)
    key_f = key_cols.astype(jnp.float32).reshape(tok_rows, kv_count, E)
    k_turned = rotate(normalize(key_f, k_gain), positions).astype(jnp.bfloat16)
    value_sel = value_cols.reshape(tok_rows, kv_count, E)
    run_max = jnp.full((kv_count, per_kv, tok_rows), -1e30, jnp.float32)
    key_block = lax.all_gather(k_turned, "sp", axis=0, tiled=True)
    value_block = lax.all_gather(value_sel, "sp", axis=0, tiled=True)
    scores = jnp.einsum(
        "qcge,kce->cgqk", q_turned, key_block, preferred_element_type=jnp.float32
    ) * E ** (-0.5)
    new_max = jnp.maximum(run_max, jnp.max(scores, axis=-1))
    exped = jnp.exp(scores - new_max[..., None])
    denominator = jnp.sum(exped, axis=-1)
    weighted = jnp.einsum(
        "cgqk,kce->cgqe",
        exped.astype(jnp.bfloat16),
        value_block,
        preferred_element_type=jnp.float32,
    )
    run_max, denominator, weighted = (new_max, denominator, weighted)
    attended = (weighted / denominator[..., None]).astype(jnp.bfloat16)
    attended = attended.transpose(2, 0, 1, 3).reshape(tok_rows, head_local * E)
    partial_value = jnp.dot(attended, out_weight, preferred_element_type=jnp.float32).astype(
        jnp.bfloat16
    )
    attn_out = lax.psum_scatter(partial_value, "tp", scatter_dimension=1, tiled=True).astype(
        jnp.float32
    )
    after_attn = residual.astype(jnp.float32) + attn_out
    square_sum = lax.psum(jnp.sum(after_attn * after_attn, axis=1), "tp")
    normed = (after_attn * lax.rsqrt(square_sum / D + norm_eps)[:, None] * norm_gain).astype(
        jnp.bfloat16
    )
    experts_n = lax.axis_size("sp")
    capacity = 5 * tok_rows * TOPK // (4 * experts_n) + 1
    assign = routes.reshape(tok_rows * TOPK)
    onehot = (assign[:, None] == jnp.arange(experts_n, dtype=jnp.int32)[None, :]).astype(jnp.int32)
    before = jnp.cumsum(onehot, axis=0) - onehot
    slot_rank = jnp.sum(before * onehot, axis=1)
    slot_index = assign * capacity + slot_rank
    token_local = jnp.arange(tok_rows * TOPK, dtype=jnp.int32) // TOPK
    slot_token = (
        jnp.full((experts_n * capacity,), tok_rows, jnp.int32).at[slot_index].set(token_local)
    )
    gate_w = w_gate[0]
    up_w = w_up[0]
    down_w = w_down[0]
    padded = jnp.concatenate([normed, jnp.zeros((1, normed.shape[1]), jnp.bfloat16)], axis=0)
    slot_rows = padded[slot_token].reshape(experts_n, capacity, normed.shape[1])
    block_rows = lax.all_gather(
        lax.all_to_all(slot_rows, "sp", split_axis=0, concat_axis=0, tiled=True),
        "tp",
        axis=2,
        tiled=True,
    )
    gate_next = jnp.einsum("scd,df->scf", block_rows, gate_w, preferred_element_type=jnp.float32)
    up_next = jnp.einsum("scd,df->scf", block_rows, up_w, preferred_element_type=jnp.float32)
    activated = (jax.nn.silu(gate_next) * up_next).astype(jnp.bfloat16)
    partials = jnp.einsum(
        "scf,fd->scd", activated, down_w, preferred_element_type=jnp.float32
    ).astype(jnp.bfloat16)
    expert_rows = (
        lax.psum_scatter(partials, "tp", scatter_dimension=2, tiled=True)
        .astype(jnp.float32)
        .astype(jnp.bfloat16)
    )
    returned_rows = lax.all_to_all(expert_rows, "sp", split_axis=0, concat_axis=0, tiled=True)
    columns = returned_rows.shape[2]
    picked = returned_rows.reshape(experts_n * capacity, columns)[slot_index].astype(jnp.float32)
    picked = picked.reshape(tok_rows, TOPK, columns)
    expert_mix = jnp.sum(picked * route_weights[:, :, None], axis=1)
    return (after_attn + expert_mix).astype(jnp.bfloat16)


def solution(mesh):
    return jax.shard_map(
        shards,
        mesh=mesh,
        in_specs=(
            P("sp", "tp"),
            P("sp", None),
            P("sp", None),
            P(),
            P(),
            P("tp", None),
            P("sp", "tp"),
            P("tp"),
            P("sp", None),
            P("sp", None),
            P("sp", None, "tp"),
            P("sp", None, "tp"),
            P("sp", "tp", None),
        ),
        out_specs=P("sp", "tp"),
        check_vma=False,
    )
```

profile of v0, /device:TPU:0, one launch (start us, length us, event | category | flops | bytes accessed | tf_op | source)
XLA Modules:
  0.0 260.0 jit_solution(18293213865418719815)
XLA Ops:
  6.5 0.0 copy-start
  6.5 0.0 reduce-scatter.3.cloned.1.call-start
  6.6 1.0 constant_dynamic-slice_fusion.1
  7.6 0.1 copy.29
  7.7 0.7 fusion.37
  8.5 0.2 multiply_cosine_fusion.1
  8.7 0.2 fusion.55
  8.9 15.9 %all_gather.9 = bf16[2048,1,64]{0,2,1:T(8,128)(2,1)S(1)} all-gather(bf16[256,1,64]{0,2,1:T(8,128)(2,1)S(1)} %pad_maximum_fusion), channel_id=1, replica_groups=mesh['sp'=8,'tp'=4] {'sp'}, dimensions={0}, use_global_device_ids=true | all-gather | bytes 294912 | tf_op jit(solution)/shard_map/all_gather | solution.py:73
  24.8 1.0 copy.20
  25.9 0.7 multiply_multiply_fusion
  26.7 0.0 copy-start.4
  26.7 4.5 %bitcast_reduce_fusion = (f32[4,256]{1,0:T(4,128)S(1)}, f32[2048,256,4]{1,0,2:T(8,128)}) fusion(bf16[256,4,16]{0,2,1:T(8,128)(2,1)S(1)} %get-tuple-element.9, bf16[256,4,16]{0,2,1:T(8,128)(2,1)S(1)} %get-tuple-element.10, bf16[256,4,16]{0,2,1:T(8,128)(2,1)S(1)} %get-tuple-element.6, bf16[256,4,16]{0,2,1:T(8,128)(2,1)S(1)} %get-tuple-element.5, ...), kind=kOutput, calls=%fused_computation.4 | convolution fusion | flops 273153024 | bytes 8785920 | tf_op jit(solution)/shard_map/qcge,kce->cgqk/dot_general | solution.py:75
  31.2 0.0 copy-done.4
  31.2 0.1 constant_dynamic-slice_fusion
  31.3 0.1 copy.28
  31.4 14.2 %all-gather = bf16[2048,64]{0,1:T(8,128)(2,1)S(1)} all-gather(bf16[256,64]{0,1:T(8,128)(2,1)S(1)} %copy.28), channel_id=2, replica_groups=mesh['sp'=8,'tp'=4] {'sp'}, dimensions={0}, use_global_device_ids=true | all-gather | bytes 294912 | tf_op jit(solution)/shard_map/all_gather | solution.py:74
  45.6 0.0 copy-start.1
  45.6 4.9 %fusion.1 = f32[4,256]{1,0:T(4,128)S(1)} fusion(f32[2048,256,4]{1,0,2:T(8,128)} %get-tuple-element.24, f32[4,256]{1,0:T(4,128)S(1)} %broadcast_maximum_fusion), kind=kLoop, calls=%fused_computation.6 | loop fusion | flops 6290432 | bytes 8396800 | tf_op jit(solution)/shard_map/reduce_sum | solution.py:80
  50.5 0.9 copy-done.1
  51.4 0.0 copy-start.5
  51.4 1.5 fusion.20
  52.9 0.0 copy-start.2
  52.9 0.0 copy-start.6
  52.9 0.0 copy-done
  52.9 1.5 convolution_convert_fusion
  54.4 0.0 reduce-scatter.3.cloned.1.call-update
  54.4 0.0 all-gather.3.cloned.1.call-start
  54.4 0.0 copy-done.5
  54.5 0.1 copy.24
  54.6 0.1 eq.32
  54.7 0.1 eq.28
  54.9 1.1 reduce-window.6
  56.0 0.2 slice_reduce_fusion
  56.3 0.1 copy.23
  56.5 0.1 mul.365
  56.6 0.1 fusion.59
  56.7 2.4 scatter_custom_fusion
  59.2 24.4 %reduce-scatter.3.cloned.1.call-done = bf16[256,512]{1,0:T(8,128)(2,1)} async-done(((bf16[256,2048]{1,0:T(8,128)(2,1)}), bf16[256,512]{1,0:T(8,128)(2,1)}) %reduce-scatter.3.cloned.1.call-update) | async-done | bytes 262160 | tf_op jit(solution)/shard_map/reduce_scatter | solution.py:93
  83.6 0.0 copy-done.2
  83.6 1.1 multiply_reduce_fusion.1
  84.7 8.9 %psum.7 = f32[256]{0:T(256)S(1)} all-reduce(f32[256]{0:T(256)S(1)} %multiply_reduce_fusion.1), channel_id=1, replica_groups=mesh['sp'=8,'tp'=4] {'tp'}, use_global_device_ids=true, to_apply=%region_6.7 | all-reduce | flops 256 | bytes 2048 | tf_op jit(solution)/shard_map/psum | solution.py:97
  93.7 0.0 copy-done.6
  93.7 1.1 multiply_convert_fusion.1
  94.8 2.8 %gather_fusion = bf16[648,512]{1,0:T(8,128)(2,1)S(1)} fusion(bf16[257,512]{1,0:T(8,128)(2,1)S(1)} %concatenate.36, s32[1024]{0:T(1024)S(1)} %pad_clamp_fusion.1), kind=kCustom, calls=%fused_computation | custom fusion | bytes 1329696 | tf_op jit(solution)/shard_map/gather | solution.py:116
  97.6 0.2 reshape.562
  97.8 24.0 %all_to_all.10 = bf16[8,81,512]{2,1,0:T(8,128)(2,1)} all-to-all(bf16[8,81,512]{2,1,0:T(8,128)(2,1)S(1)} %reshape.562), channel_id=1, replica_groups=mesh['sp'=8,'tp'=4] {'sp'}, dimensions={0} | all-to-all | bytes 1327104 | tf_op jit(solution)/shard_map/all_to_all | solution.py:118
  121.8 0.0 all-gather.3.cloned.1.call-update
  121.9 0.2 reduce-scatter.5.cloned.1.call-start
  122.1 39.4 %all-gather.3.cloned.1.call-done = bf16[8,81,2048]{2,1,0:T(8,128)(2,1)} async-done(((bf16[8,81,512]{2,1,0:T(8,128)(2,1)}), bf16[8,81,2048]{2,1,0:T(8,128)(2,1)}) %all-gather.3.cloned.1.call-update) | async-done | bytes 2654224 | tf_op jit(solution)/shard_map/all_gather | solution.py:117
  161.5 7.8 %fusion.6 = f32[8,81,1024]{2,1,0:T(8,128)} fusion(bf16[8,81,2048]{2,1,0:T(8,128)(2,1)} %all-gather.3.cloned.1.call-done, bf16[1,2048,1024]{2,1,0:T(8,128)(2,1)} %param.24), kind=kOutput, calls=%fused_computation.11 | convolution fusion | flops 2717908992 | bytes 9502720 | tf_op jit(solution)/shard_map/scd,df->scf/dot_general | solution.py:124
  169.3 13.1 %fusion.12 = bf16[8,81,2048]{2,1,0:T(8,128)(2,1)} fusion(bf16[1,1024,2048]{2,1,0:T(8,128)(2,1)} %param.25, f32[8,81,1024]{2,1,0:T(8,128)} %fusion.6, bf16[8,81,2048]{2,1,0:T(8,128)(2,1)} %all-gather.3.cloned.1.call-done, bf16[1,2048,1024]{2,1,0:T(8,128)(2,1)} %param.23), kind=kOutput, calls=%fused_computation.16 | convolution fusion | flops 5441126400 | bytes 16351232 | tf_op jit(solution)/shard_map/scf,fd->scd/dot_general | solution.py:126
  182.4 0.0 reduce-scatter.5.cloned.1.call-update
  182.4 41.9 %reduce-scatter.5.cloned.1.call-done = bf16[8,81,512]{2,1,0:T(8,128)(2,1)} async-done(((bf16[8,81,2048]{2,1,0:T(8,128)(2,1)}), bf16[8,81,512]{2,1,0:T(8,128)(2,1)}) %reduce-scatter.5.cloned.1.call-update) | async-done | bytes 663568 | tf_op jit(solution)/shard_map/reduce_scatter | solution.py:130
  224.3 4.6 %all-to-all-start.1 = ((bf16[8,81,512]{2,1,0:T(8,128)(2,1)}), bf16[8,81,512]{2,1,0:T(8,128)(2,1)S(1)}, u32[]{:S(2)}, u32[]{:S(2)}) async-start(bf16[8,81,512]{2,1,0:T(8,128)(2,1)} %reduce-scatter.5.cloned.1.call-done), calls=%async_computation.3 | async-start | bytes 1441792 | tf_op jit(solution)/shard_map/all_to_all | solution.py:134
  228.9 0.0 copy-done.7
  228.9 0.1 copy.26
  229.0 19.4 %all-to-all-done.1 = bf16[8,81,512]{2,1,0:T(8,128)(2,1)S(1)} async-done(((bf16[8,81,512]{2,1,0:T(8,128)(2,1)}), bf16[8,81,512]{2,1,0:T(8,128)(2,1)S(1)}, u32[]{:S(2)}, u32[]{:S(2)}) %all-to-all-start.1) | async-done | bytes 663584 | tf_op jit(solution)/shard_map/all_to_all | solution.py:134
  248.4 0.2 reshape.563
  248.6 0.0 copy-start.3
  248.6 2.0 gather_fusion.1
  250.6 0.7 reshape.566
  251.3 1.3 multiply_reduce_fusion
  252.6 0.0 copy-done.3
  252.6 0.8 add_convert_fusion
  (21 shorter events, 0.3 us)
Async XLA Ops:
  6.5 46.4 %copy-start = (bf16[256,2048]{1,0:T(8,128)(2,1)S(1)}, bf16[256,2048]{1,0:T(8,128)(2,1)}, u32[]{:S(2)}) copy-start(bf16[256,2048]{1,0:T(8,128)(2,1)} %param.18) | copy-start | bytes 3145732
  6.5 77.1 %reduce-scatter.3.cloned.1.call-start = ((), (), s32[]{:S(2)}) async-start(), calls=%async_computation.4 | async-start | bytes 1310720 | tf_op jit(solution)/shard_map/reduce_scatter | solution.py:93
  26.7 4.5 %copy-start.4 = (bf16[256,256]{1,0:T(8,128)(2,1)S(1)}, bf16[256,256]{1,0:T(8,128)(2,1)}, u32[]{:S(2)}) copy-start(bf16[256,256]{1,0:T(8,128)(2,1)} %param.15) | copy-start | bytes 393220
  45.6 5.8 %copy-start.1 = (f32[2048,256,4]{1,0,2:T(8,128)S(1)}, f32[2048,256,4]{1,0,2:T(8,128)}, u32[]{:S(2)}) copy-start(f32[2048,256,4]{1,0,2:T(8,128)} %get-tuple-element.24) | copy-start | bytes 25165828
  51.4 3.1 %copy-start.5 = (s32[256,2]{0,1:T(2,128)S(1)}, s32[256,2]{0,1:T(2,128)}, u32[]{:S(2)}) copy-start(s32[256,2]{0,1:T(2,128)} %param.21) | copy-start | bytes 6148
  52.9 30.7 %copy-start.2 = (bf16[256,512]{1,0:T(8,128)(2,1)S(1)}, bf16[256,512]{1,0:T(8,128)(2,1)}, u32[]{:S(2)}) copy-start(bf16[256,512]{1,0:T(8,128)(2,1)} %param.19) | copy-start | bytes 786436
  52.9 40.8 %copy-start.6 = (f32[512]{0:T(512)S(1)}, f32[512]{0:T(512)}, u32[]{:S(2)}) copy-start(f32[512]{0:T(512)} %param.20) | copy-start | bytes 6148
  54.4 107.1 %all-gather.3.cloned.1.call-start = ((), (), s32[]{:S(2)}) async-start(), calls=%async_computation.5 | async-start | bytes 3604480 | tf_op jit(solution)/shard_map/all_gather | solution.py:117
  121.9 102.4 %reduce-scatter.5.cloned.1.call-start = ((), (), s32[]{:S(2)}) async-start(), calls=%async_computation.6 | async-start | bytes 3604480 | tf_op jit(solution)/shard_map/reduce_scatter | solution.py:130
  182.4 46.5 %copy-start.7 = (f32[256,2]{0,1:T(2,128)S(1)}, f32[256,2]{0,1:T(2,128)}, u32[]{:S(2)}) copy-start(f32[256,2]{0,1:T(2,128)} %param.22) | copy-start | bytes 6148
  224.3 24.1 %all-to-all-start.1 = ((bf16[8,81,512]{2,1,0:T(8,128)(2,1)}), bf16[8,81,512]{2,1,0:T(8,128)(2,1)S(1)}, u32[]{:S(2)}, u32[]{:S(2)}) async-start(bf16[8,81,512]{2,1,0:T(8,128)(2,1)} %reduce-scatter.5.cloned.1.call-done), calls=%async_computation.3 | async-start | bytes 1441792 | tf_op jit(solution)/shard_map/all_to_all | solution.py:134
  248.6 4.0 %copy-start.3 = (bf16[256,512]{1,0:T(8,128)(2,1)S(1)}, bf16[256,512]{1,0:T(8,128)(2,1)}, u32[]{:S(2)}) copy-start(bf16[256,512]{1,0:T(8,128)(2,1)} %reduce-scatter.3.cloned.1.call-done) | copy-start | bytes 786436
Sparse Core Ops, SparseCore 0:
  54.5 29.0 reduce-scatter.2
  122.0 39.4 all-gather.2
  182.5 41.6 reduce-scatter.4
where the time goes:
time: 260 us
  waiting for transfers between devices  125 us (48%)
  blocking collectives  63.1 us (24%)
  matrix products  28.3 us (11%)
  between operations  13.4 us (5%)
  other arithmetic  12.6 us (5%)
  local copies, waits for them, and re-layouts  12.5 us (5%)
  starting transfers between devices  4.87 us (2%)
    reduce_scatter x1, waiting for transfers between devices, shards(): lax.psum_scatter(partials, 'tp', scatter_dimension=2, tiled=True)  41.9 us
    all_gather x1, waiting for transfers between devices, shards(): lax.all_gather(lax.all_to_all(slot_rows, 'sp', split_axis=0, concat_axis=...  39.4 us
    reduce_scatter x1, waiting for transfers between devices, shards(): lax.psum_scatter(partial_value, 'tp', scatter_dimension=1, tiled=True)  24.4 us
    all_to_all x1, blocking collectives, shards(): lax.all_to_all(slot_rows, 'sp', split_axis=0, concat_axis=0, tiled=True)  24 us
    all_to_all x1, waiting for transfers between devices, shards(): lax.all_to_all(expert_rows, 'sp', split_axis=0, concat_axis=0, tiled=True)  19.4 us
    all_gather x1, blocking collectives, shards(): key_block = lax.all_gather(k_turned, 'sp', axis=0, tiled=True)  15.9 us
    all_gather x1, blocking collectives, shards(): value_block = lax.all_gather(value_sel, 'sp', axis=0, tiled=True)  14.2 us
    dot_general x1, matrix products, shards(): jnp.einsum('scf,fd->scd', activated, down_w, preferred_element_type=jnp.f...  13.1 us
  transfers between devices with their start and end apart: 4, of which 4 were waited for; matrix products, arithmetic and copies ran while one was open for 2% of the time, Pallas kernels for 0%

commit v1 on v0

--- a/solution.py
+++ b/solution.py
@@ -71,7 +71,12 @@
     value_sel = value_cols.reshape(tok_rows, kv_count, E)
     run_max = jnp.full((kv_count, per_kv, tok_rows), -1e30, jnp.float32)
     key_block = lax.all_gather(k_turned, "sp", axis=0, tiled=True)
-    value_block = lax.all_gather(value_sel, "sp", axis=0, tiled=True)
+    ring = [value_sel]
+    for hop in range(7):
+        ring.append(lax.ppermute(ring[-1], "sp", [(dev, (dev + 1) % 8) for dev in range(8)]))
+    value_block = jnp.roll(
+        jnp.concatenate(ring[::-1], axis=0), (lax.axis_index("sp") + 1) * ring[0].shape[0], axis=0
+    )
     scores = jnp.einsum(
         "qcge,kce->cgqk", q_turned, key_block, preferred_element_type=jnp.float32
     ) * E ** (-0.5)

time: 260 us -> 264 us (1.015)
  waiting for transfers between devices: 125 us -> 148 us
  blocking collectives: 63.1 us -> 47.3 us
  other arithmetic: 12.6 us -> 9.04 us
    ppermute x0 -> x7, waiting for transfers between devices: none -> 25 us  [shards(): lax.ppermute(ring[-1], 'sp', [(dev, (dev + 1) % 8) for dev in range(8)])]
    all_gather x1 -> x0, blocking collectives: 14.2 us -> none  [shards(): value_block = lax.all_gather(value_sel, 'sp', axis=0, tiled=True)]
    reduce_sum x1, other arithmetic: 4.9 us -> 1.39 us  [shards(): denominator = jnp.sum(exped, axis=-1)]
    dot_general x1, matrix products: 1.52 us -> 4.9 us  [shards(): jnp.einsum('cgqk,kce->cgqe', exped.astype(jnp.bfloat16), value_block, pre...]
    dot_general x1, matrix products: 4.51 us -> 1.29 us  [shards(): jnp.einsum('qcge,kce->cgqk', q_turned, key_block, preferred_element_type=...]
  transfers between devices with their start and end apart: 4 -> 11, of which waited for: 4 -> 10; matrix products, arithmetic and copies ran while one was open for 2% -> 4% of each run, Pallas kernels for 0% -> 0%
where the time goes in v1:
time: 264 us
  waiting for transfers between devices  148 us (56%)
  blocking collectives  47.3 us (18%)
  matrix products  28.5 us (11%)
  between operations  13.5 us (5%)
  local copies, waits for them, and re-layouts  11.7 us (4%)
  other arithmetic  9.04 us (3%)
  starting transfers between devices  5.84 us (2%)
    reduce_scatter x1, waiting for transfers between devices, shards(): lax.psum_scatter(partials, 'tp', scatter_dimension=2, tiled=True)  41.9 us
    all_gather x1, waiting for transfers between devices, shards(): lax.all_gather(lax.all_to_all(slot_rows, 'sp', split_axis=0, concat_axis=...  39.4 us
    ppermute x7, waiting for transfers between devices, shards(): lax.ppermute(ring[-1], 'sp', [(dev, (dev + 1) % 8) for dev in range(8)])  25 us
    all_to_all x1, blocking collectives, shards(): lax.all_to_all(slot_rows, 'sp', split_axis=0, concat_axis=0, tiled=True)  24 us
    reduce_scatter x1, waiting for transfers between devices, shards(): lax.psum_scatter(partial_value, 'tp', scatter_dimension=1, tiled=True)  22 us
    all_to_all x1, waiting for transfers between devices, shards(): lax.all_to_all(expert_rows, 'sp', split_axis=0, concat_axis=0, tiled=True)  19.4 us
    all_gather x1, blocking collectives, shards(): key_block = lax.all_gather(k_turned, 'sp', axis=0, tiled=True)  14.3 us
    dot_general x1, matrix products, shards(): jnp.einsum('scf,fd->scd', activated, down_w, preferred_element_type=jnp.f...  13.1 us
  transfers between devices with their start and end apart: 11, of which 10 were waited for; matrix products, arithmetic and copies ran while one was open for 4% of the time, Pallas kernels for 0%

profile of v1, /device:TPU:0, one launch (start us, length us, event | category | flops | bytes accessed | tf_op | source)
XLA Modules:
  0.0 263.6 jit_solution(11071637668057635384)
XLA Ops:
  6.5 0.0 reduce-scatter.3.cloned.1.call-start
  6.5 1.1 constant_dynamic-slice_fusion
  7.6 0.1 copy.27
  7.7 0.5 collective-permute-start
  8.3 0.1 copy.28
  8.4 1.0 copy.19
  9.5 0.7 multiply_multiply_fusion
  10.2 0.2 multiply_cosine_fusion.1
  10.5 0.7 fusion.38
  11.2 2.7 %collective-permute-done = bf16[256,1,64]{0,2,1:T(8,128)(2,1)S(1)} collective-permute-done((bf16[256,1,64]{0,2,1:T(8,128)(2,1)S(1)}, bf16[256,1,64]{0,2,1:T(8,128)(2,1)S(1)}, u32[]{:S(2)}, u32[]{:S(2)}) %collective-permute-start) | collective-permute-done | bytes 32800 | tf_op jit(solution)/shard_map/ppermute | solution.py:76
  13.9 0.1 collective-permute-start.1
  13.9 0.2 fusion.56
  14.1 4.9 %collective-permute-done.1 = bf16[256,1,64]{0,2,1:T(8,128)(2,1)S(1)} collective-permute-done((bf16[256,1,64]{0,2,1:T(8,128)(2,1)S(1)}, bf16[256,1,64]{0,2,1:T(8,128)(2,1)S(1)}, u32[]{:S(2)}, u32[]{:S(2)}) %collective-permute-start.1) | collective-permute-done | bytes 32800 | tf_op jit(solution)/shard_map/ppermute | solution.py:76
  19.0 0.0 collective-permute-start.2
  19.0 5.1 %collective-permute-done.2 = bf16[256,1,64]{0,2,1:T(8,128)(2,1)S(1)} collective-permute-done((bf16[256,1,64]{0,2,1:T(8,128)(2,1)S(1)}, bf16[256,1,64]{0,2,1:T(8,128)(2,1)S(1)}, u32[]{:S(2)}, u32[]{:S(2)}) %collective-permute-start.2) | collective-permute-done | bytes 32800 | tf_op jit(solution)/shard_map/ppermute | solution.py:76
  24.2 0.0 collective-permute-start.3
  24.2 14.3 %all_gather.6 = bf16[2048,1,64]{0,2,1:T(8,128)(2,1)S(1)} all-gather(bf16[256,1,64]{0,2,1:T(8,128)(2,1)S(1)} %pad_maximum_fusion), channel_id=1, replica_groups=mesh['sp'=8,'tp'=4] {'sp'}, dimensions={0}, use_global_device_ids=true | all-gather | bytes 294912 | tf_op jit(solution)/shard_map/all_gather | solution.py:73
  38.4 0.0 collective-permute-done.3
  38.4 0.3 collective-permute-start.4
  38.8 1.3 bitcast_reduce_fusion
  40.1 3.5 %collective-permute-done.4 = bf16[256,1,64]{0,2,1:T(8,128)(2,1)S(1)} collective-permute-done((bf16[256,1,64]{0,2,1:T(8,128)(2,1)S(1)}, bf16[256,1,64]{0,2,1:T(8,128)(2,1)S(1)}, u32[]{:S(2)}, u32[]{:S(2)}) %collective-permute-start.4) | collective-permute-done | bytes 32800 | tf_op jit(solution)/shard_map/ppermute | solution.py:76
  43.6 0.0 collective-permute-start.5
  43.6 5.1 %collective-permute-done.5 = bf16[256,1,64]{0,2,1:T(8,128)(2,1)S(1)} collective-permute-done((bf16[256,1,64]{0,2,1:T(8,128)(2,1)S(1)}, bf16[256,1,64]{0,2,1:T(8,128)(2,1)S(1)}, u32[]{:S(2)}, u32[]{:S(2)}) %collective-permute-start.5) | collective-permute-done | bytes 32800 | tf_op jit(solution)/shard_map/ppermute | solution.py:76
  48.7 0.0 collective-permute-start.6
  48.7 1.4 fusion.1
  50.1 3.7 %collective-permute-done.6 = bf16[256,1,64]{0,2,1:T(8,128)(2,1)S(1)} collective-permute-done((bf16[256,1,64]{0,2,1:T(8,128)(2,1)S(1)}, bf16[256,1,64]{0,2,1:T(8,128)(2,1)S(1)}, u32[]{:S(2)}, u32[]{:S(2)}) %collective-permute-start.6) | collective-permute-done | bytes 32800 | tf_op jit(solution)/shard_map/ppermute | solution.py:76
  54.0 0.0 copy-start.4
  54.1 4.9 %fusion.20 = bf16[4,256,64]{1,2,0:T(8,128)(2,1)S(1)} fusion(f32[2048,256,4]{1,0,2:T(8,128)} %copy-done.1, f32[4,256]{1,0:T(4,128)S(1)} %broadcast_maximum_fusion, bf16[4096,1,64]{0,2,1:T(8,128)(2,1)S(1)} %constant_dynamic-update-slice_fusion, s32[]{:T(128)S(6)} %select_n.67, f32[4,256]{1,0:T(4,128)S(1)} %fusion.1), kind=kOutput, calls=%fused_computation.20 | convolution fusion | flops 274857984 | bytes 8790020 | tf_op jit(solution)/shard_map/cgqk,kce->cgqe/dot_general | solution.py:86
  59.0 0.0 copy-start.5
  59.0 0.0 copy-done
  59.0 1.5 convolution_convert_fusion
  60.4 0.0 reduce-scatter.3.cloned.1.call-update
  60.5 0.0 all-gather.2.cloned.1.call-start
  60.5 0.1 copy.23
  60.7 0.1 eq.35
  60.8 0.1 eq.31
  61.0 0.1 copy.22
  61.1 0.1 mul.369
  61.3 1.1 reduce-window.6
  62.4 0.2 slice_reduce_fusion
  62.7 0.1 fusion.60
  62.8 2.4 scatter_custom_fusion
  65.3 22.0 %reduce-scatter.3.cloned.1.call-done = bf16[256,512]{1,0:T(8,128)(2,1)} async-done(((bf16[256,2048]{1,0:T(8,128)(2,1)}), bf16[256,512]{1,0:T(8,128)(2,1)}) %reduce-scatter.3.cloned.1.call-update) | async-done | bytes 262160 | tf_op jit(solution)/shard_map/reduce_scatter | solution.py:98
  87.3 1.1 multiply_reduce_fusion.1
  88.4 8.9 %psum.7 = f32[256]{0:T(256)S(1)} all-reduce(f32[256]{0:T(256)S(1)} %multiply_reduce_fusion.1), channel_id=1, replica_groups=mesh['sp'=8,'tp'=4] {'tp'}, use_global_device_ids=true, to_apply=%region_6.7 | all-reduce | flops 256 | bytes 2048 | tf_op jit(solution)/shard_map/psum | solution.py:102
  97.3 1.1 multiply_convert_fusion.1
  98.4 2.8 %gather_fusion = bf16[648,512]{1,0:T(8,128)(2,1)S(1)} fusion(bf16[257,512]{1,0:T(8,128)(2,1)S(1)} %concatenate.43, s32[1024]{0:T(1024)S(1)} %pad_clamp_fusion.1), kind=kCustom, calls=%fused_computation | custom fusion | bytes 1329696 | tf_op jit(solution)/shard_map/gather | solution.py:121
  101.2 0.2 reshape.562
  101.5 24.0 %all_to_all.10 = bf16[8,81,512]{2,1,0:T(8,128)(2,1)} all-to-all(bf16[8,81,512]{2,1,0:T(8,128)(2,1)S(1)} %reshape.562), channel_id=1, replica_groups=mesh['sp'=8,'tp'=4] {'sp'}, dimensions={0} | all-to-all | bytes 1327104 | tf_op jit(solution)/shard_map/all_to_all | solution.py:123
  125.5 0.0 all-gather.2.cloned.1.call-update
  125.5 0.2 reduce-scatter.5.cloned.1.call-start
  125.8 39.4 %all-gather.2.cloned.1.call-done = bf16[8,81,2048]{2,1,0:T(8,128)(2,1)} async-done(((bf16[8,81,512]{2,1,0:T(8,128)(2,1)}), bf16[8,81,2048]{2,1,0:T(8,128)(2,1)}) %all-gather.2.cloned.1.call-update) | async-done | bytes 2654224 | tf_op jit(solution)/shard_map/all_gather | solution.py:122
  165.2 7.8 %fusion.6 = f32[8,81,1024]{2,1,0:T(8,128)} fusion(bf16[8,81,2048]{2,1,0:T(8,128)(2,1)} %all-gather.2.cloned.1.call-done, bf16[1,2048,1024]{2,1,0:T(8,128)(2,1)} %param.24), kind=kOutput, calls=%fused_computation.11 | convolution fusion | flops 2717908992 | bytes 9502720 | tf_op jit(solution)/shard_map/scd,df->scf/dot_general | solution.py:129
  173.0 13.1 %fusion.12 = bf16[8,81,2048]{2,1,0:T(8,128)(2,1)} fusion(bf16[1,1024,2048]{2,1,0:T(8,128)(2,1)} %param.25, f32[8,81,1024]{2,1,0:T(8,128)} %fusion.6, bf16[8,81,2048]{2,1,0:T(8,128)(2,1)} %all-gather.2.cloned.1.call-done, bf16[1,2048,1024]{2,1,0:T(8,128)(2,1)} %param.23), kind=kOutput, calls=%fused_computation.16 | convolution fusion | flops 5441126400 | bytes 16351232 | tf_op jit(solution)/shard_map/scf,fd->scd/dot_general | solution.py:131
  186.0 0.0 reduce-scatter.5.cloned.1.call-update
  186.1 41.9 %reduce-scatter.5.cloned.1.call-done = bf16[8,81,512]{2,1,0:T(8,128)(2,1)} async-done(((bf16[8,81,2048]{2,1,0:T(8,128)(2,1)}), bf16[8,81,512]{2,1,0:T(8,128)(2,1)}) %reduce-scatter.5.cloned.1.call-update) | async-done | bytes 663568 | tf_op jit(solution)/shard_map/reduce_scatter | solution.py:135
  227.9 4.6 %all-to-all-start.1 = ((bf16[8,81,512]{2,1,0:T(8,128)(2,1)}), bf16[8,81,512]{2,1,0:T(8,128)(2,1)S(1)}, u32[]{:S(2)}, u32[]{:S(2)}) async-start(bf16[8,81,512]{2,1,0:T(8,128)(2,1)} %reduce-scatter.5.cloned.1.call-done), calls=%async_computation.3 | async-start | bytes 1441792 | tf_op jit(solution)/shard_map/all_to_all | solution.py:139
  232.6 0.1 copy.25
  232.7 19.4 %all-to-all-done.1 = bf16[8,81,512]{2,1,0:T(8,128)(2,1)S(1)} async-done(((bf16[8,81,512]{2,1,0:T(8,128)(2,1)}), bf16[8,81,512]{2,1,0:T(8,128)(2,1)S(1)}, u32[]{:S(2)}, u32[]{:S(2)}) %all-to-all-start.1) | async-done | bytes 663584 | tf_op jit(solution)/shard_map/all_to_all | solution.py:139
  252.1 0.2 reshape.563
  252.3 2.0 gather_fusion.1
  254.3 0.7 reshape.566
  255.0 1.3 multiply_reduce_fusion
  256.3 0.8 add_convert_fusion
  (47 shorter events, 0.3 us)
Async XLA Ops:
  6.5 52.4 %copy-start = (bf16[256,2048]{1,0:T(8,128)(2,1)S(1)}, bf16[256,2048]{1,0:T(8,128)(2,1)}, u32[]{:S(2)}) copy-start(bf16[256,2048]{1,0:T(8,128)(2,1)} %param.18) | copy-start | bytes 3145732
  6.5 80.7 %reduce-scatter.3.cloned.1.call-start = ((), (), s32[]{:S(2)}) async-start(), calls=%async_computation.4 | async-start | bytes 1310720 | tf_op jit(solution)/shard_map/reduce_scatter | solution.py:98
  7.7 6.2 %collective-permute-start = (bf16[256,1,64]{0,2,1:T(8,128)(2,1)S(1)}, bf16[256,1,64]{0,2,1:T(8,128)(2,1)S(1)}, u32[]{:S(2)}, u32[]{:S(2)}) collective-permute-start(bf16[256,1,64]{0,2,1:T(8,128)(2,1)S(1)} %bitcast.90), channel_id=1, source_target_pairs={{0,4},{4,8},{8,12},{12,16},{16,20},{20,24},{24,28},{28,0},{1,5},{5... | collective-permute-start | bytes 98312 | tf_op jit(solution)/shard_map/ppermute | solution.py:76
  13.9 5.1 %collective-permute-start.1 = (bf16[256,1,64]{0,2,1:T(8,128)(2,1)S(1)}, bf16[256,1,64]{0,2,1:T(8,128)(2,1)S(1)}, u32[]{:S(2)}, u32[]{:S(2)}) collective-permute-start(bf16[256,1,64]{0,2,1:T(8,128)(2,1)S(1)} %collective-permute-done), channel_id=1, source_target_pairs={{0,4},{4,8},{8,12},{12,16},{16,20},{20,24},{24,28},{28,0},{1,5},{5... | collective-permute-start | bytes 98312 | tf_op jit(solution)/shard_map/ppermute | solution.py:76
  19.0 5.1 %collective-permute-start.2 = (bf16[256,1,64]{0,2,1:T(8,128)(2,1)S(1)}, bf16[256,1,64]{0,2,1:T(8,128)(2,1)S(1)}, u32[]{:S(2)}, u32[]{:S(2)}) collective-permute-start(bf16[256,1,64]{0,2,1:T(8,128)(2,1)S(1)} %collective-permute-done.1), channel_id=1, source_target_pairs={{0,4},{4,8},{8,12},{12,16},{16,20},{20,24},{24,28},{28,0},{1,5},{5... | collective-permute-start | bytes 98312 | tf_op jit(solution)/shard_map/ppermute | solution.py:76
  24.2 14.3 %collective-permute-start.3 = (bf16[256,1,64]{0,2,1:T(8,128)(2,1)S(1)}, bf16[256,1,64]{0,2,1:T(8,128)(2,1)S(1)}, u32[]{:S(2)}, u32[]{:S(2)}) collective-permute-start(bf16[256,1,64]{0,2,1:T(8,128)(2,1)S(1)} %collective-permute-done.2), channel_id=1, source_target_pairs={{0,4},{4,8},{8,12},{12,16},{16,20},{20,24},{24,28},{28,0},{1,5},{5... | collective-permute-start | bytes 98312 | tf_op jit(solution)/shard_map/ppermute | solution.py:76
  38.4 5.1 %collective-permute-start.4 = (bf16[256,1,64]{0,2,1:T(8,128)(2,1)S(1)}, bf16[256,1,64]{0,2,1:T(8,128)(2,1)S(1)}, u32[]{:S(2)}, u32[]{:S(2)}) collective-permute-start(bf16[256,1,64]{0,2,1:T(8,128)(2,1)S(1)} %collective-permute-done.3), channel_id=1, source_target_pairs={{0,4},{4,8},{8,12},{12,16},{16,20},{20,24},{24,28},{28,0},{1,5},{5... | collective-permute-start | bytes 98312 | tf_op jit(solution)/shard_map/ppermute | solution.py:76
  40.1 8.6 %copy-start.1 = (f32[2048,256,4]{1,0,2:T(8,128)}, f32[2048,256,4]{1,0,2:T(8,128)S(1)}, u32[]{:S(2)}) copy-start(f32[2048,256,4]{1,0,2:T(8,128)S(1)} %get-tuple-element.24) | copy-start | bytes 25165828
  43.6 5.1 %collective-permute-start.5 = (bf16[256,1,64]{0,2,1:T(8,128)(2,1)S(1)}, bf16[256,1,64]{0,2,1:T(8,128)(2,1)S(1)}, u32[]{:S(2)}, u32[]{:S(2)}) collective-permute-start(bf16[256,1,64]{0,2,1:T(8,128)(2,1)S(1)} %collective-permute-done.4), channel_id=1, source_target_pairs={{0,4},{4,8},{8,12},{12,16},{16,20},{20,24},{24,28},{28,0},{1,5},{5... | collective-permute-start | bytes 98312 | tf_op jit(solution)/shard_map/ppermute | solution.py:76
  48.7 5.1 %collective-permute-start.6 = (bf16[256,1,64]{0,2,1:T(8,128)(2,1)S(1)}, bf16[256,1,64]{0,2,1:T(8,128)(2,1)S(1)}, u32[]{:S(2)}, u32[]{:S(2)}) collective-permute-start(bf16[256,1,64]{0,2,1:T(8,128)(2,1)S(1)} %collective-permute-done.5), channel_id=1, source_target_pairs={{0,4},{4,8},{8,12},{12,16},{16,20},{20,24},{24,28},{28,0},{1,5},{5... | collective-permute-start | bytes 98312 | tf_op jit(solution)/shard_map/ppermute | solution.py:76
  54.0 6.5 %copy-start.4 = (s32[256,2]{0,1:T(2,128)S(1)}, s32[256,2]{0,1:T(2,128)}, u32[]{:S(2)}) copy-start(s32[256,2]{0,1:T(2,128)} %param.21) | copy-start | bytes 6148
  59.0 28.3 %copy-start.2 = (bf16[256,512]{1,0:T(8,128)(2,1)S(1)}, bf16[256,512]{1,0:T(8,128)(2,1)}, u32[]{:S(2)}) copy-start(bf16[256,512]{1,0:T(8,128)(2,1)} %param.19) | copy-start | bytes 786436
  59.0 38.4 %copy-start.5 = (f32[512]{0:T(512)S(1)}, f32[512]{0:T(512)}, u32[]{:S(2)}) copy-start(f32[512]{0:T(512)} %param.20) | copy-start | bytes 6148
  60.5 104.7 %all-gather.2.cloned.1.call-start = ((), (), s32[]{:S(2)}) async-start(), calls=%async_computation.5 | async-start | bytes 3604480 | tf_op jit(solution)/shard_map/all_gather | solution.py:122
  125.5 102.4 %reduce-scatter.5.cloned.1.call-start = ((), (), s32[]{:S(2)}) async-start(), calls=%async_computation.6 | async-start | bytes 3604480 | tf_op jit(solution)/shard_map/reduce_scatter | solution.py:135
  186.0 46.5 %copy-start.6 = (f32[256,2]{0,1:T(2,128)S(1)}, f32[256,2]{0,1:T(2,128)}, u32[]{:S(2)}) copy-start(f32[256,2]{0,1:T(2,128)} %param.22) | copy-start | bytes 6148
  227.9 24.2 %all-to-all-start.1 = ((bf16[8,81,512]{2,1,0:T(8,128)(2,1)}), bf16[8,81,512]{2,1,0:T(8,128)(2,1)S(1)}, u32[]{:S(2)}, u32[]{:S(2)}) async-start(bf16[8,81,512]{2,1,0:T(8,128)(2,1)} %reduce-scatter.5.cloned.1.call-done), calls=%async_computation.3 | async-start | bytes 1441792 | tf_op jit(solution)/shard_map/all_to_all | solution.py:139
  252.3 4.0 %copy-start.3 = (bf16[256,512]{1,0:T(8,128)(2,1)S(1)}, bf16[256,512]{1,0:T(8,128)(2,1)}, u32[]{:S(2)}) copy-start(bf16[256,512]{1,0:T(8,128)(2,1)} %reduce-scatter.3.cloned.1.call-done) | copy-start | bytes 786436
Sparse Core Ops, SparseCore 0:
  60.6 26.6 reduce-scatter.2
  125.6 39.4 all-gather.1
  186.2 41.7 reduce-scatter.4
